TPU v7x, 128 devices: a whole 4x4x4 slice. The times are simulated.
128 devices in a mesh: sp: 16 (over z, x), tp: 8 (over y, core).
Axes of the slice: x: 4, y: 4, z: 4, core: 2. Of those that a mesh axis runs over, the one named last changes fastest.
Arguments:
- x_in: bfloat16 [16, 6144, 2048], P('tp', 'sp'), may hold values from -13 to 13
- x_new: bfloat16 [16, 2048], P('sp'), may hold values from -6 to 6
- w_x: bfloat16 [2048, 2048], replicated, may hold values from -0.125 to 0.125
- w_b: bfloat16 [2048, 1024], replicated, may hold values from -0.125 to 0.125
- w_c: bfloat16 [2048, 1024], replicated, may hold values from -0.125 to 0.125
- w_dt: bfloat16 [2048, 32], replicated, may hold values from -0.125 to 0.125
- w_z: bfloat16 [2048, 2048], P(None, 'tp'), may hold values from -3 to 3
- conv_w: float32 [4, 4096], replicated, may hold values from -3 to 3
- conv_b: float32 [4096], replicated, may hold values from -3 to 3
- dt_bias: float32 [32], replicated, may hold values from -4 to -2
- a_log: float32 [32], replicated, may hold values from -12 to 0
- d_skip: float32 [32], replicated, may hold values from 1 to 8
- norm_g: float32 [32, 64], P('tp'), may hold values from 0.1 to 1.9
Outputs:
- state_cache: bfloat16 [16, 32, 64, 128], P('sp', 'tp')
- read_out: bfloat16 [16, 32, 64], P('sp', 'tp')
All inputs are finite; a program needn't handle non-finite values.
Results may differ from a plain program's by a relative error of at most 0.015.
Values may be sent and summed in bfloat16 or wider, within the bound.
A program may use at most 128 MiB of HBM per device.

v0:
```python
import jax
import jax.numpy as jnp
from jax import lax
from jax.sharding import Mesh
from jax.sharding import PartitionSpec as P

H = 32
P_SIZE = 64
G = 8
N = 128
KW = 4
R = 4
TP = ("tp_0", "tp_1")
eps = 1e-05


def copy_for_each(value, axis):
    copies = jnp.broadcast_to(value, (lax.axis_size(axis), *value.shape))
    return lax.all_to_all(copies, axis, split_axis=0, concat_axis=0, tiled=True)


def combined_pairwise(pieces, combine):
    while len(jax.tree.leaves(pieces)[0]) > 1:
        pieces = jax.vmap(combine)(*(pieces[side::2] for side in (0, 1)))
    return pieces[0]


def prefix(value, axis, combine, identity):
    devices, index = (lax.axis_size(axis), lax.axis_index(axis))
    passed = jnp.arange(devices) > index

    def kept(part, zero, own):
        part = jnp.where(
            passed.reshape(-1, *(1 for _ in own.shape)), part, jnp.asarray(zero, own.dtype)
        )
        return part[::-1]

    pieces = copy_for_each(value, axis)
    return combined_pairwise(kept(pieces, identity, value), combine)


def passed_along(value, axis, steps):
    count = lax.axis_size(axis)
    first, last = (max(0, -steps), min(count, count - steps))
    return lax.ppermute(value, axis, [(source, source + steps) for source in range(first, last)])


def broadcast(value, axis, root):
    return lax.dynamic_index_in_dim(lax.all_gather(value, axis), root, 0, keepdims=False)


def joined_along(pieces, dim):
    pieces = jnp.moveaxis(pieces, 0, dim)
    dims = pieces.shape
    return pieces.reshape(*dims[:dim], dims[dim] * dims[dim + 1], *dims[dim + 2 :])


def all_blocks(value, axes, sequence):
    pieces = value[None]
    for k in sequence:
        pieces = lax.all_gather(pieces, axes[k], axis=0, tiled=True)
    held = [lax.axis_size(axes[k]) for k in reversed(sequence)]
    pieces = pieces.reshape(*held, *value.shape)
    turned = sorted(range(len(sequence)), key=lambda place: sequence[len(sequence) - 1 - place])
    return pieces.transpose(*turned, *range(len(sequence), pieces.ndim)).reshape(-1, *value.shape)


def gather_axes(value, axes, sequence, dim):
    return joined_along(all_blocks(value, axes, sequence), dim)


def in_blocks(value, dim, devices):
    before, after = (value.shape[:dim], value.shape[dim + 1 :])
    return jnp.moveaxis(value.reshape(*before, devices, -1, *after), dim, 0)


def summed_on_arrival(value, axis, dim):
    devices = lax.axis_size(axis)
    pieces = lax.all_to_all(in_blocks(value, dim, devices), axis, 0, 0, tiled=True)
    return jnp.sum(pieces.astype(jnp.float32), axis=0)


def shift_conv(padded, weights, biases, col_count):
    acc_sum = biases + jnp.zeros(padded.shape[:1] + (col_count,) + padded.shape[2:], jnp.float32)
    for offset in range(KW):
        acc_sum = acc_sum + weights[offset] * padded[:, offset : offset + col_count].astype(
            jnp.float32
        )
    return jax.nn.silu(acc_sum).astype(jnp.bfloat16)


def project(token_rows, weight):
    flat_rows = token_rows.reshape(-1, token_rows.shape[-1])
    result = jnp.dot(flat_rows, weight, preferred_element_type=jnp.float32).astype(jnp.bfloat16)
    return result.reshape(token_rows.shape[:-1] + (weight.shape[1],))


def add_totals(earlier, later_part):
    return earlier + later_part


def decayed(step_sizes, rates, values, head_count):
    rest_sum = lax.cumsum(step_sizes, axis=1, reverse=True) - step_sizes
    totals = jnp.sum(step_sizes, axis=1)
    later_sum = prefix(totals, "sp", add_totals, jnp.zeros_like(totals))
    weight = jnp.exp(rates * (rest_sum + later_sum[:, None, :])) * step_sizes
    shaped = values.astype(jnp.float32).reshape(
        values.shape[0], values.shape[1], head_count, P_SIZE
    )
    return (weight[..., None] * shaped).astype(jnp.bfloat16)


def per_device(
    x_in, x_new, w_x, w_b, w_c, w_dt, w_z, conv_w, conv_b, dt_bias, a_log, d_skip, norm_g
):
    seq_count = x_in.shape[0]
    span_len = x_in.shape[1]
    tp_size = lax.axis_size(TP)
    sp_size = lax.axis_size("sp")
    tp_rank = lax.axis_index(TP)
    sp_rank = lax.axis_index("sp")
    heads_local = H // tp_size
    groups_local = G // tp_size
    inner_cols = H * P_SIZE
    state_cols = G * N
    edge_rows = KW - 1
    decay_rates = -jnp.exp(a_log)
    bias_local = lax.dynamic_slice_in_dim(dt_bias, tp_rank * heads_local, heads_local)
    rate_local = lax.dynamic_slice_in_dim(decay_rates, tp_rank * heads_local, heads_local)
    pre_values = project(x_in, w_x)
    pre_keys = project(x_in, w_b)
    raw_steps = project(x_in, w_dt)
    pre_query = project(x_in[:, span_len - edge_rows :], w_c)
    joined = jnp.concatenate([pre_values, pre_keys], axis=2)
    before = passed_along(joined[:, span_len - edge_rows :], "sp", 1)
    conved = shift_conv(
        jnp.concatenate([before, joined], axis=1),
        conv_w[:, : inner_cols + state_cols],
        conv_b[: inner_cols + state_cols],
        span_len,
    )
    tail_rows = jnp.concatenate([joined[:, span_len - edge_rows :], pre_query], axis=2)
    last_rows = broadcast(tail_rows, "sp", sp_size - 1)
    all_tails = gather_axes(last_rows, ("tp_0", "tp_1"), (0, 1), 0)
    step_sizes = jax.nn.softplus(raw_steps.astype(jnp.float32) + dt_bias)
    scaled = decayed(step_sizes, decay_rates, conved[..., :inner_cols], H)
    key_rows = conved[..., inner_cols:].reshape(seq_count, span_len, G, N)
    term_full = jnp.einsum(
        "slgrp,slgn->sgrpn",
        scaled.reshape(seq_count, span_len, G, R, P_SIZE),
        key_rows,
        preferred_element_type=jnp.float32,
    ).reshape(seq_count, H, P_SIZE, N)
    term_rows = lax.all_to_all(
        term_full.astype(jnp.bfloat16), TP, split_axis=1, concat_axis=0, tiled=True
    ).astype(term_full.dtype)
    state_piece = summed_on_arrival(term_rows.astype(jnp.bfloat16), "sp", 0)
    state_cache = state_piece.astype(jnp.bfloat16)
    seq_local = state_piece.shape[0]
    tails_local = lax.dynamic_slice_in_dim(all_tails, sp_rank * seq_local, seq_local, 0)
    value_cols = tp_rank * heads_local * P_SIZE
    group_cols = tp_rank * groups_local * N
    new_values = jnp.dot(
        x_new,
        lax.dynamic_slice_in_dim(w_x, value_cols, heads_local * P_SIZE, 1),
        preferred_element_type=jnp.float32,
    ).astype(jnp.bfloat16)
    new_keys = jnp.dot(
        x_new,
        lax.dynamic_slice_in_dim(w_b, group_cols, groups_local * N, 1),
        preferred_element_type=jnp.float32,
    ).astype(jnp.bfloat16)
    new_query = jnp.dot(
        x_new,
        lax.dynamic_slice_in_dim(w_c, group_cols, groups_local * N, 1),
        preferred_element_type=jnp.float32,
    ).astype(jnp.bfloat16)
    new_raw = jnp.dot(
        x_new,
        lax.dynamic_slice_in_dim(w_dt, tp_rank * heads_local, heads_local, 1),
        preferred_element_type=jnp.float32,
    ).astype(jnp.bfloat16)
    gate_new = jnp.dot(x_new, w_z, preferred_element_type=jnp.float32).astype(jnp.bfloat16)

    def new_conv(newest, col_start, col_count):
        history = lax.dynamic_slice_in_dim(tails_local, col_start, col_count, 2)
        padded = jnp.concatenate([history, newest[:, None, :]], axis=1)
        return shift_conv(
            padded,
            lax.dynamic_slice_in_dim(conv_w, col_start, col_count, 1),
            lax.dynamic_slice_in_dim(conv_b, col_start, col_count, 0),
            1,
        )[:, 0]

    conv_values = new_conv(new_values, value_cols, heads_local * P_SIZE)
    value_rows = conv_values.astype(jnp.float32).reshape(seq_local, groups_local, R, P_SIZE)
    conv_keys = new_conv(new_keys, inner_cols + group_cols, groups_local * N)
    conv_keys = conv_keys.astype(jnp.float32).reshape(seq_local, groups_local, N)
    conv_query = new_conv(new_query, inner_cols + state_cols + group_cols, groups_local * N)
    conv_query = conv_query.astype(jnp.float32).reshape(seq_local, groups_local, N)
    new_steps = jax.nn.softplus(new_raw.astype(jnp.float32) + bias_local)
    decay_new = jnp.exp(rate_local * new_steps).reshape(seq_local, groups_local, R)
    held_read = jnp.einsum(
        "sgrpn,sgn->sgrp", state_piece.reshape(seq_local, groups_local, R, P_SIZE, N), conv_query
    )
    inner_prod = jnp.sum(conv_query * conv_keys, axis=-1)
    step_group = new_steps.reshape(seq_local, groups_local, R)
    skip_local = lax.dynamic_slice_in_dim(d_skip, tp_rank * heads_local, heads_local).reshape(
        groups_local, R
    )
    output = (
        decay_new[..., None] * held_read
        + (step_group * inner_prod[:, :, None])[..., None] * value_rows
        + skip_local[None, :, :, None] * value_rows
    )
    gate_rows = gate_new.astype(jnp.float32).reshape(seq_local, groups_local, R, P_SIZE)
    gated_out = output * jax.nn.silu(gate_rows)
    group_ms = jnp.mean(gated_out * gated_out, axis=(2, 3))
    read_out = (
        gated_out
        * lax.rsqrt(group_ms + eps)[:, :, None, None]
        * norm_g.reshape(groups_local, R, P_SIZE)
    )
    read_out = read_out.astype(jnp.bfloat16).reshape(seq_local, heads_local, P_SIZE)
    return (state_cache, read_out)


def solution(mesh):
    finer = Mesh(mesh.devices.reshape(mesh.shape["sp"], 4, 2), ("sp", "tp_0", "tp_1"))
    return jax.shard_map(
        per_device,
        mesh=finer,
        in_specs=(
            P(TP, "sp", None),
            P("sp", None),
            P(),
            P(),
            P(),
            P(),
            P(None, TP),
            P(),
            P(),
            P(),
            P(),
            P(),
            P(TP, None),
        ),
        out_specs=(P("sp", TP, None, None), P("sp", TP, None)),
        check_vma=False,
    )
```

profile of v0, /device:TPU:0, one launch (start us, length us, event | category | flops | bytes accessed | tf_op | source)
XLA Modules:
  0.0 158.0 jit_solution(8769843090585375116)
XLA Ops:
  0.7 3.0 %fusion.8 = f32[768,32]{0,1:T(8,128)S(1)} fusion(bf16[768,2048]{1,0:T(8,128)(2,1)} %bitcast.261, bf16[2048,32]{0,1:T(8,128)(2,1)} %param.18), kind=kOutput, calls=%fused_computation.16 | convolution fusion | flops 100712448 | bytes 3375104 | tf_op jit(solution)/shard_map/dot_general | solution.py:94
  3.7 0.2 fusion.77
  3.9 0.6 broadcast_in_dim.21
  4.5 8.0 %all-to-all-start = ((f32[16,2,32]{2,1,0:T(2,128)}), f32[16,2,32]{2,1,0:T(2,128)S(1)}, u32[]{:S(2)}, u32[]{:S(2)}) async-start(f32[16,2,32]{2,1,0:T(2,128)} %broadcast_in_dim.21), calls=%async_computation | async-start | bytes 32768 | tf_op jit(solution)/shard_map/all_to_all | solution.py:19
  12.5 7.7 %convolution_convert_fusion.1 = bf16[768,1024]{1,0:T(8,128)(2,1)} fusion(bf16[768,2048]{1,0:T(8,128)(2,1)} %bitcast.262, bf16[2048,1024]{1,0:T(8,128)(2,1)} %param.16), kind=kOutput, calls=%fused_computation.12 | convolution fusion | flops 3222011904 | bytes 8912896 | tf_op jit(solution)/shard_map/dot_general | solution.py:94
  20.2 1.9 %copy.66 = bf16[2,384,1024]{1,2,0:T(8,128)(2,1)S(1)} copy(bf16[2,384,1024]{2,1,0:T(8,128)(2,1)} %bitcast.267) | data formatting | bytes 3145728 | tf_op jit(solution)/shard_map/reshape | solution.py:95
  22.1 11.9 %convolution_convert_fusion = bf16[768,2048]{1,0:T(8,128)(2,1)} fusion(bf16[768,2048]{1,0:T(8,128)(2,1)} %bitcast.263, bf16[2048,2048]{1,0:T(8,128)(2,1)} %param.15), kind=kOutput, calls=%fused_computation.7 | convolution fusion | flops 6444023808 | bytes 14680064 | tf_op jit(solution)/shard_map/dot_general | solution.py:94
  34.0 4.6 %copy.65 = bf16[2,384,2048]{1,2,0:T(8,128)(2,1)} copy(bf16[2,384,2048]{2,1,0:T(8,128)(2,1)} %bitcast.265) | data formatting | bytes 6291456 | tf_op jit(solution)/shard_map/reshape | solution.py:95
  38.6 2.9 %fusion.4 = bf16[2,3,3072]{1,2,0:T(8,128)(2,1)} fusion(bf16[2,384,2048]{1,2,0:T(8,128)(2,1)} %copy.65, bf16[2,384,1024]{1,2,0:T(8,128)(2,1)S(1)} %copy.66), kind=kLoop, calls=%fused_computation.13 | loop fusion | flops 73728 | bytes 4755456 | tf_op jit(solution)/shard_map/concatenate | solution.py:134
  41.6 2.4 %copy.67 = bf16[2,3,3072]{2,0,1:T(2,128)(2,1)} copy(bf16[2,3,3072]{1,2,0:T(8,128)(2,1)} %fusion.4) | data formatting | bytes 73728 | tf_op jit(solution)/shard_map/slice | solution.py:135
  43.9 4.0 %collective-permute-start = (bf16[2,3,3072]{2,0,1:T(2,128)(2,1)}, bf16[2,3,3072]{2,0,1:T(2,128)(2,1)S(1)}, u32[]{:S(2)}, u32[]{:S(2)}) collective-permute-start(bf16[2,3,3072]{2,0,1:T(2,128)(2,1)} %copy.67), channel_id=1, source_target_pairs={{0,8},{8,16},{16,24},{24,32},{32,40},{40,48},{48,56},{56,64},{64,7... | collective-permute-start | bytes 110600 | tf_op jit(solution)/shard_map/ppermute | solution.py:45
  47.9 0.9 slice.168
  48.8 0.6 exponential_negate_fusion
  49.5 2.8 %convolution_convert_fusion.3 = bf16[6,1024]{1,0:T(8,128)(2,1)S(1)} fusion(bf16[6,2048]{1,0:T(8,128)(2,1)S(1)} %reshape.243, bf16[2048,1024]{1,0:T(8,128)(2,1)} %param.17), kind=kOutput, calls=%fused_computation.17 | convolution fusion | flops 25171968 | bytes 4231168 | tf_op jit(solution)/shard_map/dot_general | solution.py:94
  52.4 7.5 %reduce-window.6 = f32[2,32,3,128]{3,1,2,0:T(8,128)S(1)} reduce-window(f32[2,32,3,128]{3,1,2,0:T(8,128)S(1)} %bitcast.276, f32[]{:T(128)} %constant.97.clone.1), window={size=1x1x1x128 pad=0_0x0_0x0_0x0_127}, to_apply=%region_0.1 | reduce-window | flops 3121152 | bytes 196612 | tf_op jit(solution)/shard_map/reduce-window
  59.9 0.1 copy.62
  60.0 0.3 copy.74
  60.3 3.2 %pad_maximum_fusion.1 = bf16[2,3,4096]{1,2,0:T(8,128)(2,1)} fusion(bf16[2,3,1024]{1,2,0:T(8,128)(2,1)S(1)} %copy.74, bf16[2,3,3072]{1,2,0:T(8,128)(2,1)} %fusion.4), kind=kLoop, calls=%fused_computation.10 | loop fusion | flops 98304 | bytes 98304 | tf_op jit(solution)/shard_map/concatenate | solution.py:142
  63.5 0.8 fusion.32
  64.3 0.6 dynamic_slice.68
  64.9 0.7 dynamic-slice.6
  65.8 0.8 fusion.30
  66.7 1.6 %copy.68 = bf16[2,3,3072]{1,2,0:T(8,128)(2,1)} copy(bf16[2,3,3072]{2,0,1:T(2,128)(2,1)S(1)} %collective-permute-done) | data formatting | bytes 73728 | tf_op jit(solution)/shard_map/ppermute | solution.py:45
  68.3 8.2 %maximum_maximum_fusion = bf16[2,387,3072]{1,2,0:T(8,128)(2,1)S(1)} fusion(bf16[2,384,1024]{1,2,0:T(8,128)(2,1)S(1)} %copy.66, bf16[2,384,2048]{1,2,0:T(8,128)(2,1)} %copy.65, bf16[2,3,3072]{1,2,0:T(8,128)(2,1)} %copy.68), kind=kLoop, calls=%fused_computation.1 | loop fusion | flops 14266368 | bytes 9510912 | tf_op jit(solution)/shard_map/concatenate | solution.py:137
  76.5 10.8 %multiply_convert_fusion = bf16[2,384,3072]{1,2,0:T(8,128)(2,1)S(1)} fusion(bf16[2,384,1024]{1,2,0:T(8,128)(2,1)S(1)} %copy.66, bf16[2,384,2048]{1,2,0:T(8,128)(2,1)S(1)} %copy-done.1, bf16[2,387,3072]{1,2,0:T(8,128)(2,1)S(1)} %maximum_maximum_fusion, f32[3072]{0:T(1024)S(1)} %bitcast.279, f32[3072]{0:T(1024)S(1)} %bitcast.280, f32[3072]{0:T(1024)S(1)} %bitcast.281, ...), kind=kLoop, calls=%fused_computation | loop fusion | flops 47185920 | bytes 23654400 | tf_op jit(solution)/shard_map/convert_element_type | solution.py:89
  87.4 0.2 slice.200
  87.5 0.3 slice.199
  87.9 1.0 fusion.5
  88.9 1.1 copy.70
  90.0 4.6 %all-to-all-start.1 = ((bf16[2,32,64,128]{3,2,0,1:T(8,128)(2,1)}), bf16[2,32,64,128]{3,2,0,1:T(8,128)(2,1)}, u32[]{:S(2)}, u32[]{:S(2)}) async-start(bf16[2,32,64,128]{3,2,0,1:T(8,128)(2,1)} %copy.70), calls=%async_computation.1 | async-start | bytes 2097152 | tf_op jit(solution)/shard_map/all_to_all | solution.py:154
  94.7 0.9 copy.75
  95.6 25.1 %all-gather = bf16[32,3,4096]{2,1,0:T(4,128)(2,1)S(1)} all-gather(bf16[2,3,4096]{2,1,0:T(4,128)(2,1)S(1)} %copy.75), channel_id=2, replica_groups=mesh['sp'=16,'tp_0'=4,'tp_1'=2] {'sp'}, dimensions={0}, use_global_device_ids=true | all-gather | bytes 835584 | tf_op jit(solution)/shard_map/all_gather | solution.py:49
  120.7 12.7 %all-gather.1 = bf16[8,3,4096]{2,1,0:T(4,128)(2,1)S(1)} all-gather(bf16[2,3,4096]{2,1,0:T(4,128)(2,1)S(1)} %slice.201), channel_id=3, replica_groups=mesh['sp'=16,'tp_0'=4,'tp_1'=2] {'tp_0'}, dimensions={0}, use_global_device_ids=true | all-gather | bytes 245760 | tf_op jit(solution)/shard_map/all_gather | solution.py:61
  133.4 0.2 copy.76
  133.6 1.5 fusion.22
  135.1 2.3 %copy.72 = bf16[8,2,4,64,128]{4,3,2,1,0:T(8,128)(2,1)} copy(bf16[8,2,4,64,128]{4,3,1,2,0:T(8,128)(2,1)} %bitcast.17) | data formatting | bytes 2097152 | tf_op jit(solution)/shard_map/all_to_all | solution.py:154
  137.5 4.9 %all-to-all-start.2 = ((bf16[16,1,4,64,128]{4,3,2,1,0:T(8,128)(2,1)}), bf16[16,1,4,64,128]{4,3,2,1,0:T(8,128)(2,1)S(1)}, u32[]{:S(2)}, u32[]{:S(2)}) async-start(bf16[16,1,4,64,128]{4,3,2,1,0:T(8,128)(2,1)} %bitcast.19), calls=%async_computation.2 | async-start | bytes 2097152 | tf_op jit(solution)/shard_map/all_to_all | solution.py:79
  142.4 2.1 %all_gather.15 = bf16[8,2,3,4096]{3,1,2,0:T(2,128)(2,1)S(1)} all-gather(bf16[4,2,3,4096]{3,1,2,0:T(2,128)(2,1)S(1)} %copy.76), channel_id=1, replica_groups=mesh['sp'=16,'tp_0'=4,'tp_1'=2] {'tp_1'}, dimensions={0}, use_global_device_ids=true | all-gather | bytes 589824 | tf_op jit(solution)/shard_map/all_gather | solution.py:61
  144.5 0.3 copy.77
  144.9 0.1 convert_reduce_fusion.1
  145.2 1.2 divide_multiply_fusion.3
  146.5 1.9 %multiply_reduce_fusion.1 = f32[]{:T(128)} fusion(bf16[1,2048]{1,0:T(2,128)(2,1)S(1)} %copy-done.4, bf16[2048,1024]{1,0:T(8,128)(2,1)} %param.16, s32[]{:T(128)S(6)} %select_n.62, f32[4,128]{1,0:T(4,128)S(1)} %get-tuple-element.9, bf16[1,3,128]{2,1,0:T(4,128)(2,1)S(1)} %get-tuple-element.5, f32[4096]{0:T(1024)S(1)} %copy-done.6, s32[]{:T(128)S(6)} %select_n.63, ...), kind=kOutput, calls=%fused_computation.113 | convolution fusion | flops 527103 | bytes 531980 | tf_op jit(solution)/shard_map/dot_general | solution.py:168
  148.3 1.5 multiply_exponential_fusion
  149.9 5.9 %all-to-all-done.2 = bf16[16,1,4,64,128]{4,3,2,1,0:T(8,128)(2,1)S(1)} async-done(((bf16[16,1,4,64,128]{4,3,2,1,0:T(8,128)(2,1)}), bf16[16,1,4,64,128]{4,3,2,1,0:T(8,128)(2,1)S(1)}, u32[]{:S(2)}, u32[]{:S(2)}) %all-to-all-start.2) | async-done | bytes 1048608 | tf_op jit(solution)/shard_map/all_to_all | solution.py:79
  155.7 0.2 convert_reduce_fusion
  155.9 0.1 fusion.56
  156.1 0.7 multiply_reduce_fusion
  157.5 0.6 fusion.45
  (60 shorter events, 0.7 us)
Async XLA Ops:
  0.6 62.9 %copy-start = (bf16[2048,256]{1,0:T(8,128)(2,1)S(1)}, bf16[2048,256]{1,0:T(8,128)(2,1)}, u32[]{:S(2)}) copy-start(bf16[2048,256]{1,0:T(8,128)(2,1)} %param.19) | copy-start | bytes 3145732
  0.6 3.0 %copy-start.10 = (f32[32]{0:T(128)S(1)}, f32[32]{0:T(128)}, u32[]{:S(2)}) copy-start(f32[32]{0:T(128)} %param.22) | copy-start | bytes 388
  4.5 61.1 %all-to-all-start = ((f32[16,2,32]{2,1,0:T(2,128)}), f32[16,2,32]{2,1,0:T(2,128)S(1)}, u32[]{:S(2)}, u32[]{:S(2)}) async-start(f32[16,2,32]{2,1,0:T(2,128)} %broadcast_in_dim.21), calls=%async_computation | async-start | bytes 32768 | tf_op jit(solution)/shard_map/all_to_all | solution.py:19
  38.6 10.2 %copy-start.14 = (f32[32]{0:T(128)S(1)}, f32[32]{0:T(128)}, u32[]{:S(2)}) copy-start(f32[32]{0:T(128)} %param.23) | copy-start | bytes 388
  41.6 10.8 %copy-start.5 = (f32[4,4096]{1,0:T(4,128)S(1)}, f32[4,4096]{1,0:T(4,128)}, u32[]{:S(2)}) copy-start(f32[4,4096]{1,0:T(4,128)} %param.20) | copy-start | bytes 196612
  43.9 22.7 %collective-permute-start = (bf16[2,3,3072]{2,0,1:T(2,128)(2,1)}, bf16[2,3,3072]{2,0,1:T(2,128)(2,1)S(1)}, u32[]{:S(2)}, u32[]{:S(2)}) collective-permute-start(bf16[2,3,3072]{2,0,1:T(2,128)(2,1)} %copy.67), channel_id=1, source_target_pairs={{0,8},{8,16},{16,24},{24,32},{32,40},{40,48},{48,56},{56,64},{64,7... | collective-permute-start | bytes 110600 | tf_op jit(solution)/shard_map/ppermute | solution.py:45
  49.5 14.1 %copy-start.4 = (bf16[1,2048]{1,0:T(2,128)(2,1)S(1)}, bf16[1,2048]{1,0:T(2,128)(2,1)}, u32[]{:S(2)}) copy-start(bf16[1,2048]{1,0:T(2,128)(2,1)} %param.14) | copy-start | bytes 12292
  52.3 12.0 %copy-start.6 = (f32[4096]{0:T(1024)S(1)}, f32[4096]{0:T(1024)}, u32[]{:S(2)}) copy-start(f32[4096]{0:T(1024)} %param.21) | copy-start | bytes 49156
  68.3 8.2 %copy-start.1 = (bf16[2,384,2048]{1,2,0:T(8,128)(2,1)S(1)}, bf16[2,384,2048]{1,2,0:T(8,128)(2,1)}, u32[]{:S(2)}) copy-start(bf16[2,384,2048]{1,2,0:T(8,128)(2,1)} %copy.65) | copy-start | bytes 9437188
  68.3 8.2 %slice-start = ((f32[4096]{0:T(1024)}), f32[3072]{0:T(1024)S(1)}, s32[]{:S(2)}) async-start(f32[4096]{0:T(1024)} %param.21), calls=%async_computation.3 | async-start | bytes 24576 | tf_op jit(solution)/shard_map/slice | solution.py:139
  87.8 6.7 %copy-start.7 = (f32[1,256]{1,0:T(1,128)S(1)}, f32[1,256]{1,0:T(1,128)}, u32[]{:S(2)}) copy-start(f32[1,256]{1,0:T(1,128)} %fusion.32) | copy-start | bytes 3076
  87.9 6.8 %copy-start.2 = (bf16[2,3,4096]{1,2,0:T(8,128)(2,1)S(1)}, bf16[2,3,4096]{1,2,0:T(8,128)(2,1)}, u32[]{:S(2)}) copy-start(bf16[2,3,4096]{1,2,0:T(8,128)(2,1)} %pad_maximum_fusion.1) | copy-start | bytes 147460
  90.0 45.1 %copy-start.8 = (f32[1,256]{1,0:T(1,128)S(1)}, f32[1,256]{1,0:T(1,128)}, u32[]{:S(2)}) copy-start(f32[1,256]{1,0:T(1,128)} %dynamic-slice.6) | copy-start | bytes 3076
  90.0 45.2 %all-to-all-start.1 = ((bf16[2,32,64,128]{3,2,0,1:T(8,128)(2,1)}), bf16[2,32,64,128]{3,2,0,1:T(8,128)(2,1)}, u32[]{:S(2)}, u32[]{:S(2)}) async-start(bf16[2,32,64,128]{3,2,0,1:T(8,128)(2,1)} %copy.70), calls=%async_computation.1 | async-start | bytes 2097152 | tf_op jit(solution)/shard_map/all_to_all | solution.py:154
  95.6 49.3 %copy-start.9 = (f32[256]{0:T(256)S(1)}, f32[256]{0:T(256)}, u32[]{:S(2)}) copy-start(f32[256]{0:T(256)} %dynamic_slice.68) | copy-start | bytes 3076
  95.6 49.5 %copy-start.15 = (f32[32]{0:T(128)S(1)}, f32[32]{0:T(128)}, u32[]{:S(2)}) copy-start(f32[32]{0:T(128)} %param.24) | copy-start | bytes 388
  133.4 14.9 %copy-start.11 = (f32[32]{0:T(128)S(1)}, f32[32]{0:T(128)}, u32[]{:S(2)}) copy-start(f32[32]{0:T(128)} %param.22) | copy-start | bytes 388
  133.4 14.9 %copy-start.13 = (f32[32]{0:T(128)S(1)}, f32[32]{0:T(128)}, u32[]{:S(2)}) copy-start(f32[32]{0:T(128)} %exponential_negate_fusion) | copy-start | bytes 388
  135.1 22.3 %copy-start.12 = (f32[4,64]{1,0:T(4,128)S(1)}, f32[4,64]{1,0:T(4,128)}, u32[]{:S(2)}) copy-start(f32[4,64]{1,0:T(4,128)} %param.25) | copy-start | bytes 3076
  137.5 18.3 %all-to-all-start.2 = ((bf16[16,1,4,64,128]{4,3,2,1,0:T(8,128)(2,1)}), bf16[16,1,4,64,128]{4,3,2,1,0:T(8,128)(2,1)S(1)}, u32[]{:S(2)}, u32[]{:S(2)}) async-start(bf16[16,1,4,64,128]{4,3,2,1,0:T(8,128)(2,1)} %bitcast.19), calls=%async_computation.2 | async-start | bytes 2097152 | tf_op jit(solution)/shard_map/all_to_all | solution.py:79
  155.9 2.1 %copy-start.3 = (bf16[4,64,128]{2,1,0:T(8,128)(2,1)}, bf16[4,64,128]{2,1,0:T(8,128)(2,1)S(1)}, u32[]{:S(2)}) copy-start(bf16[4,64,128]{2,1,0:T(8,128)(2,1)S(1)} %convert_reduce_fusion) | copy-start | bytes 196612
where the time goes:
time: 159 us; the launch traced here: 158 us
  blocking collectives  39.8 us (25%)
  other arithmetic  35.9 us (23%)
  matrix products  33.5 us (21%)
  starting transfers between devices  21.5 us (14%)
  local copies, waits for them, and re-layouts  19.6 us (12%)
  waiting for transfers between devices  5.88 us (4%)
  between operations  1.71 us (1%)
    dot_general x4, matrix products, project(): jnp.dot(flat_rows, weight, preferred_element_type=jnp.float32)  25.4 us
    all_gather x1, blocking collectives, broadcast(): lax.all_gather(value, axis)  25.1 us
    all_gather x2, blocking collectives, all_blocks(): pieces = lax.all_gather(pieces, axes[k], axis=0, tiled=True)  14.8 us
    convert_element_type x1, other arithmetic, shift_conv(): return jax.nn.silu(acc_sum).astype(jnp.bfloat16)  10.8 us
    concatenate x1, other arithmetic, per_device(): jnp.concatenate([before, joined], axis=1)  8.2 us
    all_to_all x1, starting transfers between devices, copy_for_each(): return lax.all_to_all(copies, axis, split_axis=0, concat_axis=0, tiled=True)  7.99 us
    another operation x2, other arithmetic  7.5 us
    reshape x4, local copies, waits for them, and re-layouts, project(): return result.reshape(token_rows.shape[:-1] + (weight.shape[1],))  6.86 us
  transfers between devices with their start and end apart: 4, of which 1 were waited for; matrix products, arithmetic and copies ran while one was open for 37% of the time, Pallas kernels for 0%

commit v1 on v0

--- a/solution.py
+++ b/solution.py
@@ -58,7 +58,9 @@
 def all_blocks(value, axes, sequence):
     pieces = value[None]
     for k in sequence:
-        pieces = lax.all_gather(pieces, axes[k], axis=0, tiled=True)
+        pieces = jnp.concatenate(
+            lax.all_to_all(jnp.stack([pieces] * lax.axis_size(axes[k])), axes[k], 0, 0), axis=0
+        )
     held = [lax.axis_size(axes[k]) for k in reversed(sequence)]
     pieces = pieces.reshape(*held, *value.shape)
     turned = sorted(range(len(sequence)), key=lambda place: sequence[len(sequence) - 1 - place])

time: 159 us -> 174 us (1.094)
  waiting for transfers between devices: 5.88 us -> 25.9 us
  blocking collectives: 39.8 us -> 26.3 us
  starting transfers between devices: 21.5 us -> 29.5 us
    all_gather x2 -> x0, blocking collectives: 14.8 us -> none  [all_blocks(): pieces = lax.all_gather(pieces, axes[k], axis=0, tiled=True)]
    all_to_all x1, waiting for transfers between devices: 0.01 us -> 12.9 us  [per_device(): lax.all_to_all(term_full.astype(jnp.bfloat16), TP, split_axis=1, concat_a...]
    all_to_all x0 -> x2, starting transfers between devices: none -> 7.93 us  [all_blocks(): lax.all_to_all(jnp.stack([pieces] * lax.axis_size(axes[k])), axes[k], 0, 0)]
    all_to_all x1, waiting for transfers between devices: 5.87 us -> 12.5 us  [summed_on_arrival(): lax.all_to_all(in_blocks(value, dim, devices), axis, 0, 0, tiled=True)]
    another operation x2 -> x4, local copies, waits for them, and re-layouts: 0.01 us -> 1.91 us  [the longest x2 1.9 us: all_blocks(): jnp.stack([pieces] * lax.axis_size(axes[k]))]
    another operation x2 -> x3, other arithmetic: 7.5 us -> 7.86 us
  transfers between devices with their start and end apart: 4 -> 6, of which waited for: 1 -> 3; matrix products, arithmetic and copies ran while one was open for 37% -> 49% of each run, Pallas kernels for 0% -> 0%
where the time goes in v1:
time: 174 us; the launch traced here: 173 us
  other arithmetic  35.5 us (20%)
  matrix products  32.9 us (19%)
  starting transfers between devices  29.5 us (17%)
  blocking collectives  26.3 us (15%)
  waiting for transfers between devices  25.9 us (15%)
  local copies, waits for them, and re-layouts  20.9 us (12%)
    all_gather x1, blocking collectives, broadcast(): lax.all_gather(value, axis)  26.3 us
    dot_general x4, matrix products, project(): jnp.dot(flat_rows, weight, preferred_element_type=jnp.float32)  25.4 us
    all_to_all x1, waiting for transfers between devices, per_device(): lax.all_to_all(term_full.astype(jnp.bfloat16), TP, split_axis=1, concat_a...  12.9 us
    all_to_all x1, waiting for transfers between devices, summed_on_arrival(): lax.all_to_all(in_blocks(value, dim, devices), axis, 0, 0, tiled=True)  12.5 us
    convert_element_type x1, other arithmetic, shift_conv(): return jax.nn.silu(acc_sum).astype(jnp.bfloat16)  10.8 us
    concatenate x1, other arithmetic, per_device(): jnp.concatenate([before, joined], axis=1)  8.2 us
    all_to_all x1, starting transfers between devices, copy_for_each(): return lax.all_to_all(copies, axis, split_axis=0, concat_axis=0, tiled=True)  7.99 us
    all_to_all x2, starting transfers between devices, all_blocks(): lax.all_to_all(jnp.stack([pieces] * lax.axis_size(axes[k])), axes[k], 0, 0)  7.93 us
  transfers between devices with their start and end apart: 6, of which 3 were waited for; matrix products, arithmetic and copies ran while one was open for 49% of the time, Pallas kernels for 0%

profile of v1, /device:TPU:0, one launch (start us, length us, event | category | flops | bytes accessed | tf_op | source)
XLA Modules:
  0.0 172.8 jit_solution(12102890703735285609)
XLA Ops:
  0.7 3.0 %fusion.8 = f32[768,32]{0,1:T(8,128)S(1)} fusion(bf16[768,2048]{1,0:T(8,128)(2,1)} %bitcast.259, bf16[2048,32]{0,1:T(8,128)(2,1)} %param.18), kind=kOutput, calls=%fused_computation.16 | convolution fusion | flops 100712448 | bytes 3375104 | tf_op jit(solution)/shard_map/dot_general | solution.py:96
  3.7 0.2 fusion.77
  3.9 0.6 broadcast_in_dim.21
  4.5 8.0 %all-to-all-start = ((f32[16,2,32]{2,1,0:T(2,128)}), f32[16,2,32]{2,1,0:T(2,128)S(1)}, u32[]{:S(2)}, u32[]{:S(2)}) async-start(f32[16,2,32]{2,1,0:T(2,128)} %broadcast_in_dim.21), calls=%async_computation | async-start | bytes 32768 | tf_op jit(solution)/shard_map/all_to_all | solution.py:19
  12.5 7.7 %convolution_convert_fusion.1 = bf16[768,1024]{1,0:T(8,128)(2,1)} fusion(bf16[768,2048]{1,0:T(8,128)(2,1)} %bitcast.260, bf16[2048,1024]{1,0:T(8,128)(2,1)} %param.16), kind=kOutput, calls=%fused_computation.12 | convolution fusion | flops 3222011904 | bytes 8912896 | tf_op jit(solution)/shard_map/dot_general | solution.py:96
  20.2 1.9 %copy.65 = bf16[2,384,1024]{1,2,0:T(8,128)(2,1)S(1)} copy(bf16[2,384,1024]{2,1,0:T(8,128)(2,1)} %bitcast.266) | data formatting | bytes 3145728 | tf_op jit(solution)/shard_map/reshape | solution.py:97
  22.1 11.9 %convolution_convert_fusion = bf16[768,2048]{1,0:T(8,128)(2,1)} fusion(bf16[768,2048]{1,0:T(8,128)(2,1)} %bitcast.261, bf16[2048,2048]{1,0:T(8,128)(2,1)} %param.15), kind=kOutput, calls=%fused_computation.7 | convolution fusion | flops 6444023808 | bytes 14680064 | tf_op jit(solution)/shard_map/dot_general | solution.py:96
  34.0 4.6 %copy.64 = bf16[2,384,2048]{1,2,0:T(8,128)(2,1)} copy(bf16[2,384,2048]{2,1,0:T(8,128)(2,1)} %bitcast.264) | data formatting | bytes 6291456 | tf_op jit(solution)/shard_map/reshape | solution.py:97
  38.6 2.9 %fusion.4 = bf16[2,3,3072]{1,2,0:T(8,128)(2,1)} fusion(bf16[2,384,2048]{1,2,0:T(8,128)(2,1)} %copy.64, bf16[2,384,1024]{1,2,0:T(8,128)(2,1)S(1)} %copy.65), kind=kLoop, calls=%fused_computation.13 | loop fusion | flops 73728 | bytes 4755456 | tf_op jit(solution)/shard_map/concatenate | solution.py:136
  41.6 2.4 %copy.66 = bf16[2,3,3072]{2,0,1:T(2,128)(2,1)} copy(bf16[2,3,3072]{1,2,0:T(8,128)(2,1)} %fusion.4) | data formatting | bytes 73728 | tf_op jit(solution)/shard_map/slice | solution.py:137
  43.9 3.8 %collective-permute-start = (bf16[2,3,3072]{2,0,1:T(2,128)(2,1)}, bf16[2,3,3072]{2,0,1:T(2,128)(2,1)S(1)}, u32[]{:S(2)}, u32[]{:S(2)}) collective-permute-start(bf16[2,3,3072]{2,0,1:T(2,128)(2,1)} %copy.66), channel_id=1, source_target_pairs={{0,8},{8,16},{16,24},{24,32},{32,40},{40,48},{48,56},{56,64},{64,7... | collective-permute-start | bytes 110600 | tf_op jit(solution)/shard_map/ppermute | solution.py:45
  47.8 0.9 slice.168
  48.6 0.5 exponential_negate_fusion
  49.2 2.8 %convolution_convert_fusion.3 = bf16[6,1024]{1,0:T(8,128)(2,1)S(1)} fusion(bf16[6,2048]{1,0:T(8,128)(2,1)S(1)} %reshape.244, bf16[2048,1024]{1,0:T(8,128)(2,1)} %param.17), kind=kOutput, calls=%fused_computation.17 | convolution fusion | flops 25171968 | bytes 4231168 | tf_op jit(solution)/shard_map/dot_general | solution.py:96
  52.2 7.5 %reduce-window.6 = f32[2,32,3,128]{3,1,2,0:T(8,128)S(1)} reduce-window(f32[2,32,3,128]{3,1,2,0:T(8,128)S(1)} %bitcast.275, f32[]{:T(128)} %constant.97.clone.1), window={size=1x1x1x128 pad=0_0x0_0x0_0x0_127}, to_apply=%region_0.1 | reduce-window | flops 3121152 | bytes 196612 | tf_op jit(solution)/shard_map/reduce-window
  59.8 0.3 copy.73
  60.1 3.2 %pad_maximum_fusion.1 = bf16[2,3,4096]{1,2,0:T(8,128)(2,1)} fusion(bf16[2,3,1024]{1,2,0:T(8,128)(2,1)S(1)} %copy.73, bf16[2,3,3072]{1,2,0:T(8,128)(2,1)} %fusion.4), kind=kLoop, calls=%fused_computation.10 | loop fusion | flops 98304 | bytes 98304 | tf_op jit(solution)/shard_map/concatenate | solution.py:144
  63.3 2.0 %copy.74 = bf16[2,3,4096]{2,1,0:T(4,128)(2,1)S(1)} copy(bf16[2,3,4096]{1,2,0:T(8,128)(2,1)} %pad_maximum_fusion.1) | data formatting | bytes 98304 | tf_op jit(solution)/shard_map/concatenate | solution.py:144
  65.3 26.3 %all-gather = bf16[32,3,4096]{2,1,0:T(4,128)(2,1)} all-gather(bf16[2,3,4096]{2,1,0:T(4,128)(2,1)S(1)} %copy.74), channel_id=2, replica_groups=mesh['sp'=16,'tp_0'=4,'tp_1'=2] {'sp'}, dimensions={0}, use_global_device_ids=true | all-gather | bytes 835584 | tf_op jit(solution)/shard_map/all_gather | solution.py:49
  91.6 0.2 fusion.32
  92.0 0.9 slice.201
  92.9 0.8 stack.6
  93.8 4.5 %all-to-all-start.3 = ((bf16[4,1,2,3,4096]{4,2,3,1,0:T(2,128)(2,1)}), bf16[4,1,2,3,4096]{4,2,3,1,0:T(2,128)(2,1)S(1)}, u32[]{:S(2)}, u32[]{:S(2)}) async-start(bf16[4,1,2,3,4096]{4,2,3,1,0:T(2,128)(2,1)} %stack.6), calls=%async_computation.3 | async-start | bytes 393216 | tf_op jit(solution)/shard_map/all_to_all | solution.py:62
  98.4 0.2 fusion.30
  98.6 1.6 copy.67
  100.2 8.2 %maximum_maximum_fusion = bf16[2,387,3072]{1,2,0:T(8,128)(2,1)S(1)} fusion(bf16[2,384,1024]{1,2,0:T(8,128)(2,1)S(1)} %copy.65, bf16[2,384,2048]{1,2,0:T(8,128)(2,1)} %copy.64, bf16[2,3,3072]{1,2,0:T(8,128)(2,1)} %copy.67), kind=kLoop, calls=%fused_computation.1 | loop fusion | flops 14266368 | bytes 9510912 | tf_op jit(solution)/shard_map/concatenate | solution.py:139
  108.5 10.8 %multiply_convert_fusion = bf16[2,384,3072]{1,2,0:T(8,128)(2,1)S(1)} fusion(bf16[2,384,1024]{1,2,0:T(8,128)(2,1)S(1)} %copy.65, bf16[2,384,2048]{1,2,0:T(8,128)(2,1)S(1)} %copy-done.1, bf16[2,387,3072]{1,2,0:T(8,128)(2,1)S(1)} %maximum_maximum_fusion, f32[3072]{0:T(1024)S(1)} %bitcast.278, f32[3072]{0:T(1024)S(1)} %bitcast.279, f32[3072]{0:T(1024)S(1)} %bitcast.280, ...), kind=kLoop, calls=%fused_computation | loop fusion | flops 47185920 | bytes 23654400 | tf_op jit(solution)/shard_map/convert_element_type | solution.py:91
  119.3 0.2 slice.200
  119.5 0.3 slice.199
  119.8 1.0 fusion.5
  120.8 1.1 copy.69
  121.9 4.8 %all-to-all-start.1 = ((bf16[2,32,64,128]{3,2,0,1:T(8,128)(2,1)}), bf16[2,32,64,128]{3,2,0,1:T(8,128)(2,1)S(1)}, u32[]{:S(2)}, u32[]{:S(2)}) async-start(bf16[2,32,64,128]{3,2,0,1:T(8,128)(2,1)} %copy.69), calls=%async_computation.1 | async-start | bytes 2097152 | tf_op jit(solution)/shard_map/all_to_all | solution.py:156
  126.9 1.5 fusion.22
  128.3 0.4 pad_maximum_fusion.2
  128.7 1.1 copy.76
  129.8 12.9 %all-to-all-done.1 = bf16[2,32,64,128]{3,2,0,1:T(8,128)(2,1)S(1)} async-done(((bf16[2,32,64,128]{3,2,0,1:T(8,128)(2,1)}), bf16[2,32,64,128]{3,2,0,1:T(8,128)(2,1)S(1)}, u32[]{:S(2)}, u32[]{:S(2)}) %all-to-all-start.1) | async-done | bytes 1048608 | tf_op jit(solution)/shard_map/all_to_all | solution.py:156
  142.6 3.5 %all-to-all-start.4 = ((bf16[2,4,2,3,4096]{4,1,3,2,0:T(4,128)(2,1)}), bf16[2,4,2,3,4096]{4,1,3,2,0:T(4,128)(2,1)S(1)}, u32[]{:S(2)}, u32[]{:S(2)}) async-start(bf16[2,4,2,3,4096]{4,1,3,2,0:T(4,128)(2,1)} %copy.76), calls=%async_computation.4 | async-start | bytes 786432 | tf_op jit(solution)/shard_map/all_to_all | solution.py:62
  146.1 1.1 copy.71
  147.2 0.6 all-to-all-done.4
  147.7 5.0 %all-to-all-start.2 = ((bf16[16,1,4,64,128]{4,3,2,1,0:T(8,128)(2,1)}), bf16[16,1,4,64,128]{4,3,2,1,0:T(8,128)(2,1)S(1)}, u32[]{:S(2)}, u32[]{:S(2)}) async-start(bf16[16,1,4,64,128]{4,3,2,1,0:T(8,128)(2,1)} %bitcast.19), calls=%async_computation.2 | async-start | bytes 2097152 | tf_op jit(solution)/shard_map/all_to_all | solution.py:81
  152.7 0.3 copy.77
  153.3 1.2 divide_multiply_fusion.3
  154.6 1.9 %multiply_reduce_fusion.1 = f32[]{:T(128)} fusion(bf16[1,2048]{1,0:T(2,128)(2,1)S(1)} %copy-done.3, bf16[2048,1024]{1,0:T(8,128)(2,1)} %param.16, s32[]{:T(128)S(6)} %select_n.62, f32[4,128]{1,0:T(4,128)S(1)} %get-tuple-element.9, bf16[1,3,128]{2,1,0:T(4,128)(2,1)S(1)} %get-tuple-element.5, f32[4096]{0:T(1024)S(1)} %copy-done.5, s32[]{:T(128)S(6)} %select_n.63, ...), kind=kOutput, calls=%fused_computation.114 | convolution fusion | flops 527103 | bytes 531980 | tf_op jit(solution)/shard_map/dot_general | solution.py:170
  156.4 1.5 multiply_exponential_fusion
  158.0 12.5 %all-to-all-done.2 = bf16[16,1,4,64,128]{4,3,2,1,0:T(8,128)(2,1)S(1)} async-done(((bf16[16,1,4,64,128]{4,3,2,1,0:T(8,128)(2,1)}), bf16[16,1,4,64,128]{4,3,2,1,0:T(8,128)(2,1)S(1)}, u32[]{:S(2)}, u32[]{:S(2)}) %all-to-all-start.2) | async-done | bytes 1048608 | tf_op jit(solution)/shard_map/all_to_all | solution.py:81
  170.5 0.2 convert_reduce_fusion
  170.8 0.7 multiply_reduce_fusion
  172.2 0.6 fusion.45
  (57 shorter events, 1.3 us)
Async XLA Ops:
  0.6 90.9 %copy-start = (bf16[2048,256]{1,0:T(8,128)(2,1)S(1)}, bf16[2048,256]{1,0:T(8,128)(2,1)}, u32[]{:S(2)}) copy-start(bf16[2048,256]{1,0:T(8,128)(2,1)} %param.19) | copy-start | bytes 3145732
  0.6 3.0 %copy-start.6 = (f32[32]{0:T(128)S(1)}, f32[32]{0:T(128)}, u32[]{:S(2)}) copy-start(f32[32]{0:T(128)} %param.22) | copy-start | bytes 388
  4.5 88.4 %all-to-all-start = ((f32[16,2,32]{2,1,0:T(2,128)}), f32[16,2,32]{2,1,0:T(2,128)S(1)}, u32[]{:S(2)}, u32[]{:S(2)}) async-start(f32[16,2,32]{2,1,0:T(2,128)} %broadcast_in_dim.21), calls=%async_computation | async-start | bytes 32768 | tf_op jit(solution)/shard_map/all_to_all | solution.py:19
  38.6 10.0 %copy-start.10 = (f32[32]{0:T(128)S(1)}, f32[32]{0:T(128)}, u32[]{:S(2)}) copy-start(f32[32]{0:T(128)} %param.23) | copy-start | bytes 388
  41.6 10.5 %copy-start.4 = (f32[4,4096]{1,0:T(4,128)S(1)}, f32[4,4096]{1,0:T(4,128)}, u32[]{:S(2)}) copy-start(f32[4,4096]{1,0:T(4,128)} %param.20) | copy-start | bytes 196612
  43.9 54.7 %collective-permute-start = (bf16[2,3,3072]{2,0,1:T(2,128)(2,1)}, bf16[2,3,3072]{2,0,1:T(2,128)(2,1)S(1)}, u32[]{:S(2)}, u32[]{:S(2)}) collective-permute-start(bf16[2,3,3072]{2,0,1:T(2,128)(2,1)} %copy.66), channel_id=1, source_target_pairs={{0,8},{8,16},{16,24},{24,32},{32,40},{40,48},{48,56},{56,64},{64,7... | collective-permute-start | bytes 110600 | tf_op jit(solution)/shard_map/ppermute | solution.py:45
  52.1 39.4 %copy-start.3 = (bf16[1,2048]{1,0:T(2,128)(2,1)S(1)}, bf16[1,2048]{1,0:T(2,128)(2,1)}, u32[]{:S(2)}) copy-start(bf16[1,2048]{1,0:T(2,128)(2,1)} %param.14) | copy-start | bytes 12292
  60.1 31.7 %copy-start.5 = (f32[4096]{0:T(1024)S(1)}, f32[4096]{0:T(1024)}, u32[]{:S(2)}) copy-start(f32[4096]{0:T(1024)} %param.21) | copy-start | bytes 49156
  63.3 35.1 %copy-start.7 = (f32[32]{0:T(128)S(1)}, f32[32]{0:T(128)}, u32[]{:S(2)}) copy-start(f32[32]{0:T(128)} %param.22) | copy-start | bytes 388
  63.3 35.1 %copy-start.9 = (f32[32]{0:T(128)S(1)}, f32[32]{0:T(128)}, u32[]{:S(2)}) copy-start(f32[32]{0:T(128)} %exponential_negate_fusion) | copy-start | bytes 388
  93.8 28.1 %all-to-all-start.3 = ((bf16[4,1,2,3,4096]{4,2,3,1,0:T(2,128)(2,1)}), bf16[4,1,2,3,4096]{4,2,3,1,0:T(2,128)(2,1)S(1)}, u32[]{:S(2)}, u32[]{:S(2)}) async-start(bf16[4,1,2,3,4096]{4,2,3,1,0:T(2,128)(2,1)} %stack.6), calls=%async_computation.3 | async-start | bytes 393216 | tf_op jit(solution)/shard_map/all_to_all | solution.py:62
  100.2 8.2 %copy-start.1 = (bf16[2,384,2048]{1,2,0:T(8,128)(2,1)S(1)}, bf16[2,384,2048]{1,2,0:T(8,128)(2,1)}, u32[]{:S(2)}) copy-start(bf16[2,384,2048]{1,2,0:T(8,128)(2,1)} %copy.64) | copy-start | bytes 9437188
  100.2 8.2 %slice-start = ((f32[4096]{0:T(1024)}), f32[3072]{0:T(1024)S(1)}, s32[]{:S(2)}) async-start(f32[4096]{0:T(1024)} %param.21), calls=%async_computation.5 | async-start | bytes 24576 | tf_op jit(solution)/shard_map/slice | solution.py:141
  119.8 7.0 %copy-start.11 = (f32[32]{0:T(128)S(1)}, f32[32]{0:T(128)}, u32[]{:S(2)}) copy-start(f32[32]{0:T(128)} %param.24) | copy-start | bytes 388
  121.9 20.7 %all-to-all-start.1 = ((bf16[2,32,64,128]{3,2,0,1:T(8,128)(2,1)}), bf16[2,32,64,128]{3,2,0,1:T(8,128)(2,1)S(1)}, u32[]{:S(2)}, u32[]{:S(2)}) async-start(bf16[2,32,64,128]{3,2,0,1:T(8,128)(2,1)} %copy.69), calls=%async_computation.1 | async-start | bytes 2097152 | tf_op jit(solution)/shard_map/all_to_all | solution.py:156
  129.8 42.4 %copy-start.8 = (f32[4,64]{1,0:T(4,128)S(1)}, f32[4,64]{1,0:T(4,128)}, u32[]{:S(2)}) copy-start(f32[4,64]{1,0:T(4,128)} %param.25) | copy-start | bytes 3076
  142.6 5.1 %all-to-all-start.4 = ((bf16[2,4,2,3,4096]{4,1,3,2,0:T(4,128)(2,1)}), bf16[2,4,2,3,4096]{4,1,3,2,0:T(4,128)(2,1)S(1)}, u32[]{:S(2)}, u32[]{:S(2)}) async-start(bf16[2,4,2,3,4096]{4,1,3,2,0:T(4,128)(2,1)} %copy.76), calls=%async_computation.4 | async-start | bytes 786432 | tf_op jit(solution)/shard_map/all_to_all | solution.py:62
  147.7 22.8 %all-to-all-start.2 = ((bf16[16,1,4,64,128]{4,3,2,1,0:T(8,128)(2,1)}), bf16[16,1,4,64,128]{4,3,2,1,0:T(8,128)(2,1)S(1)}, u32[]{:S(2)}, u32[]{:S(2)}) async-start(bf16[16,1,4,64,128]{4,3,2,1,0:T(8,128)(2,1)} %bitcast.19), calls=%async_computation.2 | async-start | bytes 2097152 | tf_op jit(solution)/shard_map/all_to_all | solution.py:81
  170.7 2.1 %copy-start.2 = (bf16[4,64,128]{2,1,0:T(8,128)(2,1)}, bf16[4,64,128]{2,1,0:T(8,128)(2,1)S(1)}, u32[]{:S(2)}) copy-start(bf16[4,64,128]{2,1,0:T(8,128)(2,1)S(1)} %convert_reduce_fusion) | copy-start | bytes 196612
